TPU v7x, 32 devices: a whole 2x2x4 slice. The times are simulated.
32 devices in a mesh: grp: 2 (over y), dp: 2 (over x), kv: 4 (over z), tp: 2 (over core).
Axes of the slice: x: 2, y: 2, z: 4, core: 2. Of those that a mesh axis runs over, the one named last changes fastest.
Arguments:
- candidate_vectors: bfloat16 [128, 4, 2048], P(('grp', 'dp'), None, ('kv', 'tp')), parts along dimension 0, may hold values from -6 to 6
- leading_scaling_factor: bfloat16 [2048], replicated, may hold values from 0.099609375 to 1.8984375
- lane_feed_matrix: bfloat16 [2048, 32, 2, 64], P(None, 'kv', 'tp')
- final_valve_matrix: bfloat16 [2048, 32, 2, 64], P(None, 'kv', 'tp'), may hold values from -0.125 to 0.125
- increment_matrix: bfloat16 [2048, 32, 2], replicated, may hold values from -0.125 to 0.125
- entry_basis_matrix: bfloat16 [2048, 2, 128], P(None, 'tp'), may hold values from -0.125 to 0.125
- readout_basis_matrix: bfloat16 [2048, 2, 128], P(None, 'tp'), may hold values from -0.125 to 0.125
- lane_feed_kernel: float32 [4, 32, 2, 64], P(None, 'kv', 'tp'), may hold values from -3 to 3
- entry_basis_kernel: float32 [4, 2, 128], P(None, 'tp'), may hold values from -3 to 3
- readout_basis_kernel: float32 [4, 2, 128], P(None, 'tp'), may hold values from -3 to 3
- increment_offset: float32 [32, 2], P('kv', 'tp'), may hold values from -4 to 1
- shrink_speed_exponent: float32 [32, 2], P('kv', 'tp'), may hold values from 0 to 2.8
- lane_bypass_factor: float32 [32, 2], P('kv', 'tp'), may hold values from 0.5 to 1.5
- final_linear_matrix: bfloat16 [32, 2, 64, 2048], P(None, None, None, ('kv', 'tp')), may hold values from -0.09375 to 0.09375
- hidden_carried_memory: float32 [128, 32, 2, 64, 128], P(('grp', 'dp'), 'kv', 'tp'), parts along dimension 0, may hold values from -0.6 to 0.6
- lane_filter_memory: bfloat16 [128, 7, 32, 2, 64], P(('grp', 'dp'), None, 'kv', 'tp'), parts along dimension 0, may hold values from -6 to 6
- entry_basis_memory: bfloat16 [128, 7, 2, 128], P(('grp', 'dp'), None, 'tp'), parts along dimension 0, may hold values from -6 to 6
- readout_basis_memory: bfloat16 [128, 7, 2, 128], P(('grp', 'dp'), None, 'tp'), parts along dimension 0, may hold values from -6 to 6
- predecessor_index: int32 [128, 4], P(('grp', 'dp')), parts along dimension 0, may hold values from -1 to 2, as said below
- admitted_counts: int32 [128], P(('grp', 'dp')), parts along dimension 0, may hold values from 0 to 4
- surplus_fading: float32 [128, 4, 32, 2], P(('grp', 'dp'), None, 'kv', 'tp'), parts along dimension 0, may hold values from -0.7 to 0, as said below
Outputs:
- mixed: bfloat16 [128, 4, 2048], P(('grp', 'dp'), None, ('kv', 'tp')), parts along dimension 0
There are 2 independent parts, one for each index of `grp`. A program takes and returns all parts, laid end to end along the dimension named above; an argument that names none is the same for every part. Nothing has to cross between parts.
Inputs may be any that keep to these rules, and one draw needn't show every extreme that they name: predecessor_index[s, j] is -1 or a smaller proposal index than j. `surplus_fading`: zero except at a few proposals and heads.
All inputs are finite; a program needn't handle non-finite values.
Results may differ from a plain program's by a relative error of at most 0.012.
Values may be sent and summed in bfloat16 or wider, within the bound.
A program may use at most 64 MiB of HBM per device.

v0:
```python
import jax
import jax.numpy as jnp
from jax import lax
from jax.sharding import PartitionSpec as P

D = 2048
HG = 32
G = 2
HD = 64
N = 128
CONV = 4
WIN = 7
HIGH = lax.Precision.HIGHEST


def lineage_tables(predecessor_index):
    seqs, props = predecessor_index.shape
    column = jnp.arange(props, dtype=jnp.int32)
    current = jnp.broadcast_to(column[None, :], (seqs, props))
    depth = jnp.zeros((seqs, props), jnp.int32)
    onehots = []
    for step in range(props):
        onehots.append((current[:, :, None] == column[None, None, :]).astype(jnp.float32))
        if step > 0:
            depth = depth + (current >= 0).astype(jnp.int32)
        upward = jnp.take_along_axis(predecessor_index, jnp.maximum(current, 0), axis=1)
        current = jnp.where(current >= 0, upward, -1)
    return (onehots, depth)


def conv_tree(current, saved, taps, onehots, depth, admitted_counts):
    slots = jnp.arange(saved.shape[1], dtype=jnp.int32)
    cur_f = current.astype(jnp.float32)
    saved_f = saved.astype(jnp.float32)
    total = jnp.zeros(cur_f.shape, jnp.float32)
    for lag in range(CONV):
        value = jnp.einsum("sji,sic->sjc", onehots[lag], cur_f, precision=HIGH)
        target = admitted_counts[:, None] + (CONV - 1) - (lag - depth)
        chosen = ((depth < lag)[:, :, None] & (slots[None, None, :] == target[:, :, None])).astype(
            jnp.float32
        )
        value = value + jnp.einsum("sjw,swc->sjc", chosen, saved_f, precision=HIGH)
        total = total + taps[CONV - 1 - lag] * value
    return jax.nn.silu(total)


def shards(
    candidate_vectors,
    leading_scaling_factor,
    lane_feed_matrix,
    final_valve_matrix,
    increment_matrix,
    entry_basis_matrix,
    readout_basis_matrix,
    lane_feed_kernel,
    entry_basis_kernel,
    readout_basis_kernel,
    increment_offset,
    shrink_speed_exponent,
    lane_bypass_factor,
    final_linear_matrix,
    hidden_carried_memory,
    lane_filter_memory,
    entry_basis_memory,
    readout_basis_memory,
    predecessor_index,
    admitted_counts,
    surplus_fading,
):
    seqs, props, feat_dev = candidate_vectors.shape
    heads_dev = increment_offset.shape[0]
    rows = seqs * props
    kv_index = lax.axis_index("kv")
    tp_index = lax.axis_index("tp")
    dt_own = lax.dynamic_slice(
        increment_matrix, (0, kv_index * heads_dev, tp_index), (D, heads_dev, 1)
    ).reshape(D, heads_dev)
    wx_flat = lane_feed_matrix.reshape(D, heads_dev * HD)
    wz_flat = final_valve_matrix.reshape(D, heads_dev * HD)
    wb_flat = entry_basis_matrix.reshape(D, N)
    wc_flat = readout_basis_matrix.reshape(D, N)
    piece = lax.all_gather(candidate_vectors, ("kv", "tp"), axis=2, tiled=True)
    width = piece.shape[2]
    piece_f = piece.astype(jnp.float32)
    gain = leading_scaling_factor.astype(jnp.float32)
    scaled = (piece_f * gain).astype(jnp.bfloat16).reshape(rows, width)

    def partial_dot(source, weight):
        return jnp.dot(source, weight, preferred_element_type=jnp.float32)

    x_acc = partial_dot(scaled, wx_flat)
    z_acc = partial_dot(scaled, wz_flat)
    dt_acc = partial_dot(scaled, dt_own)
    b_acc = partial_dot(scaled, wb_flat)
    c_acc = partial_dot(scaled, wc_flat)
    squares = jnp.sum(piece_f * piece_f, axis=2).reshape(rows)
    r_in = lax.rsqrt(squares / D + 1e-06)
    x_rows = (x_acc * r_in[:, None]).astype(jnp.bfloat16).reshape(seqs, props, heads_dev * HD)
    z_rows = (z_acc * r_in[:, None]).astype(jnp.bfloat16).reshape(seqs, props, heads_dev, 1, HD)
    dt_raw = (dt_acc * r_in[:, None]).reshape(seqs, props, heads_dev, 1)
    b_flat = (b_acc * r_in[:, None]).astype(jnp.bfloat16)
    c_flat = (c_acc * r_in[:, None]).astype(jnp.bfloat16)
    onehots, depth = lineage_tables(predecessor_index)
    x_conv = conv_tree(
        x_rows,
        lane_filter_memory.reshape(seqs, WIN, -1),
        lane_feed_kernel.reshape(CONV, -1),
        onehots,
        depth,
        admitted_counts,
    ).reshape(seqs, props, heads_dev, 1, HD)
    b_conv = conv_tree(
        b_flat.reshape(seqs, props, N),
        entry_basis_memory.reshape(seqs, WIN, N),
        entry_basis_kernel.reshape(CONV, N),
        onehots,
        depth,
        admitted_counts,
    ).reshape(seqs, props, 1, N)
    c_conv = conv_tree(
        c_flat.reshape(seqs, props, N),
        readout_basis_memory.reshape(seqs, WIN, N),
        readout_basis_kernel.reshape(CONV, N),
        onehots,
        depth,
        admitted_counts,
    ).reshape(seqs, props, 1, N)
    lineage = sum(onehots)
    lane_increment = jax.nn.softplus(dt_raw + increment_offset)
    fading_exponent = -jnp.exp(shrink_speed_exponent) * lane_increment + surplus_fading
    level = jnp.einsum("sji,sihg->sjhg", lineage, fading_exponent, precision=HIGH)
    gap = level[:, :, None] - level[:, None, :]
    weight = jnp.where(lineage[:, :, :, None, None] > 0, jnp.exp(jnp.minimum(gap, 0.0)), 0.0)
    scores = jnp.einsum("sjgn,sign->sjig", c_conv, b_conv, precision=HIGH)
    mixing = weight * scores[:, :, :, None, :] * lane_increment[:, None]
    y_rows = jnp.einsum("sjihg,sihgp->sjhgp", mixing, x_conv, precision=HIGH)
    y_rows = y_rows + jnp.exp(level)[..., None] * jnp.einsum(
        "shgpn,sjgn->sjhgp", hidden_carried_memory, c_conv, precision=HIGH
    )
    y_rows = y_rows + lane_bypass_factor[..., None] * x_conv
    gated = (
        (y_rows * jax.nn.silu(z_rows.astype(jnp.float32)))
        .astype(jnp.bfloat16)
        .reshape(rows, heads_dev * HD)
    )
    kv_count = lax.axis_size("kv")
    out_cols = final_linear_matrix.shape[3]
    out_flat = jnp.transpose(
        final_linear_matrix.reshape(kv_count, heads_dev, G, HD, out_cols), (0, 2, 1, 3, 4)
    ).reshape(HG * G * HD, out_cols)
    empty = jnp.zeros((rows, out_cols), jnp.float32)
    gated_f = gated.astype(jnp.float32)
    sumsq_start = lax.psum(jnp.sum(gated_f * gated_f, axis=1), ("kv", "tp"))
    product = jnp.dot(
        lax.all_gather(gated, ("kv", "tp"), axis=1, tiled=True),
        out_flat,
        preferred_element_type=jnp.float32,
    )
    sumsq = (empty, sumsq_start)[1]
    r_out = lax.rsqrt(sumsq / (HG * G * HD) + 1e-05)
    return (product * r_out[:, None]).astype(jnp.bfloat16).reshape(seqs, props, out_cols)


def solution(mesh):
    placed = (
        P(("grp", "dp"), None, ("kv", "tp")),
        P(),
        P(None, "kv", "tp", None),
        P(None, "kv", "tp", None),
        P(),
        P(None, "tp", None),
        P(None, "tp", None),
        P(None, "kv", "tp", None),
        P(None, "tp", None),
        P(None, "tp", None),
        P("kv", "tp"),
        P("kv", "tp"),
        P("kv", "tp"),
        P(None, None, None, ("kv", "tp")),
        P(("grp", "dp"), "kv", "tp", None, None),
        P(("grp", "dp"), None, "kv", "tp", None),
        P(("grp", "dp"), None, "tp", None),
        P(("grp", "dp"), None, "tp", None),
        P(("grp", "dp"), None),
        P(("grp", "dp")),
        P(("grp", "dp"), None, "kv", "tp"),
    )
    return jax.shard_map(
        shards,
        mesh=mesh,
        in_specs=placed,
        out_specs=P(("grp", "dp"), None, ("kv", "tp")),
        check_vma=False,
    )
```

profile of v0, /device:TPU:0, one launch (start us, length us, event | category | flops | bytes accessed | tf_op | source)
XLA Modules:
  0.0 125.6 jit_solution(8136422851500246056)
XLA Ops:
  6.8 0.5 copy-done.1
  7.4 1.5 %gather_fusion = s32[128]{0:T(128)S(1)} fusion(s32[32,4]{0,1:T(4,128)S(1)} %copy-done.1, s32[128]{0:T(128)S(1)} %reshape.376), kind=kCustom, calls=%fused_computation.clone | custom fusion | bytes 2048 | tf_op jit(solution)/shard_map/jit(take_along_axis)/gather | solution.py:26
  9.2 0.1 reshape.381
  9.4 1.5 %gather_fusion.1 = s32[128]{0:T(128)S(1)} fusion(s32[32,4]{0,1:T(4,128)S(1)} %copy-done.1, s32[128]{0:T(128)S(1)} %reshape.381), kind=kCustom, calls=%fused_computation.1.clone | custom fusion | bytes 2048 | tf_op jit(solution)/shard_map/jit(take_along_axis)/gather | solution.py:26
  11.2 0.1 reshape.386
  11.3 1.5 %gather_fusion.2 = s32[128]{0:T(128)S(1)} fusion(s32[32,4]{0,1:T(4,128)S(1)} %copy-done.1, s32[128]{0:T(128)S(1)} %reshape.386), kind=kCustom, calls=%fused_computation.2.clone | custom fusion | bytes 2048 | tf_op jit(solution)/shard_map/jit(take_along_axis)/gather | solution.py:26
  13.3 15.4 %all_gather.6 = bf16[32,4,2048]{2,1,0:T(4,128)(2,1)S(1)} all-gather(bf16[32,4,256]{2,1,0:T(4,128)(2,1)S(1)} %copy-done.7), channel_id=1, replica_groups=mesh['grp'=2,'dp'=2,'kv'=4,'tp'=2] {'kv','tp'}, dimensions={2}, use_global_device_ids=true | all-gather | bytes 589824 | tf_op jit(solution)/shard_map/all_gather | solution.py:82
  28.7 0.5 fusion.30
  29.4 0.1 reshape.317
  29.5 1.3 %fusion.27 = bf16[128,128]{1,0:T(8,128)(2,1)S(1)} fusion(bf16[128,2048]{1,0:T(8,128)(2,1)S(1)} %reshape.317, bf16[2048,1,128]{2,0,1:T(8,128)(2,1)} %param.28, f32[128]{0:T(128)S(1)} %rsqrt.14), kind=kOutput, calls=%fused_computation.50 | convolution fusion | flops 67141632 | bytes 1081856 | tf_op jit(solution)/shard_map/dot_general | solution.py:89
  30.9 0.9 fusion.67
  31.7 0.9 fusion.70
  32.6 0.8 fusion.90
  33.3 0.9 fusion.73
  34.2 0.8 fusion.76
  35.0 1.3 %fusion.28 = bf16[128,128]{1,0:T(8,128)(2,1)S(1)} fusion(bf16[128,2048]{1,0:T(8,128)(2,1)S(1)} %reshape.317, bf16[2048,1,128]{2,0,1:T(8,128)(2,1)} %param.29, f32[128]{0:T(128)S(1)} %rsqrt.14), kind=kOutput, calls=%fused_computation.51 | convolution fusion | flops 67141632 | bytes 1081856 | tf_op jit(solution)/shard_map/dot_general | solution.py:89
  36.3 0.9 fusion.66
  37.2 0.9 fusion.69
  38.0 0.8 fusion.72
  38.9 0.8 fusion.75
  39.7 0.8 fusion.9
  40.6 1.0 fusion.68
  41.5 0.3 fusion.71
  41.8 1.0 fusion.74
  42.8 0.2 fusion.77
  43.0 0.1 copy.129
  43.5 0.7 copy.134
  44.8 1.3 %reshape.391 = bf16[32,7,512]{2,1,0:T(8,128)(2,1)S(1)} reshape(bf16[32,7,8,1,64]{4,2,3,1,0:T(8,128)(2,1)} %param.38) | data formatting | bytes 458752 | tf_op jit(solution)/shard_map/reshape | solution.py:106
  46.1 0.3 fusion.8
  46.4 1.2 fusion.7
  47.7 0.3 fusion.5
  48.0 0.4 divide_multiply_fusion
  48.4 0.2 reshape.333
  48.6 1.0 reshape.321
  49.6 1.2 negate_bitcast_fusion
  50.9 0.6 slice_bitcast_fusion.4
  51.5 0.6 slice_bitcast_fusion
  52.1 0.9 constant_dynamic-slice_fusion
  53.1 0.2 convolution_multiply_fusion.5
  53.3 0.1 copy.137
  53.6 0.9 copy.151
  54.5 1.1 fusion.26
  55.7 1.1 fusion.25
  56.8 1.1 fusion.23
  57.9 1.2 fusion.21
  59.0 1.1 fusion.19
  60.2 0.3 fusion.18
  60.4 0.3 fusion.16
  60.7 0.3 divide_multiply_fusion.1
  61.0 0.4 convolution_bitcast_fusion
  61.4 0.9 copy.149
  62.3 1.7 %fusion.124 = (f32[32,4,8]{2,1,0:T(4,128)}, f32[32,4,8]{2,1,0:T(4,128)S(1)}) fusion(f32[32,4,8,1]{2,1,0,3:T(4,128)S(1)} %copy.138, f32[32,4,8,1]{2,1,0,3:T(4,128)S(1)} %bitcast.125, f32[8]{0:T(128)S(1)} %bitcast.135, f32[8]{0:T(128)} %negate_bitcast_fusion, s32[32,4]{1,0:T(8,128)S(1)} %copy.132, s32[32,4]{1,0:T(8,128)S(1)} %copy.128, s32[32,4]{1,0:T(8,128)S(1)} %copy.124), kind=kOutput, calls=%fused_computation.189 | convolution fusion | flops 64000 | bytes 17984 | tf_op jit(solution)/shard_map/sji,sihg->sjhg/dot_general | solution.py:131
  64.1 0.3 copy.139
  64.3 2.4 %fusion.11 = f32[128,512]{1,0:T(8,128)S(1)} fusion(bf16[128,2048]{1,0:T(8,128)(2,1)S(1)} %reshape.317, bf16[2048,512]{0,1:T(8,128)(2,1)} %bitcast.122, f32[128]{0:T(128)S(1)} %rsqrt.14), kind=kOutput, calls=%fused_computation.22 | convolution fusion | flops 268632064 | bytes 2884096 | tf_op jit(solution)/shard_map/dot_general | solution.py:89
  66.8 0.9 reshape.341
  67.7 22.1 %fusion = f32[32,4,8,64]{3,1,2,0:T(4,128)S(1)} fusion(f32[32,8,1,64,128]{4,3,2,1,0:T(8,128)} %param.37, f32[32,4,128]{2,1,0:T(4,128)} %copy-done.6), kind=kOutput, calls=%fused_computation.3 | convolution fusion | flops 100663296 | bytes 8716288 | tf_op jit(solution)/shard_map/shgpn,sjgn->sjhgp/dot_general | solution.py:137
  89.9 2.1 %fusion.36 = f32[32,8,64,4]{2,3,1,0:T(4,128)S(1)} fusion(f32[32,4,8,64]{3,2,1,0:T(8,128)S(1)} %copy-done.3, f32[32,4,8]{1,2,0:T(8,128)S(1)} %copy-done.5, f32[32,4,4]{2,1,0:T(4,128)S(1)} %copy-done.10, f32[32,4,8]{1,2,0:T(8,128)S(1)} %copy.139, pred[32,4,4]{2,1,0:T(4,128)(4,1)S(1)} %copy-done.15), kind=kOutput, calls=%fused_computation.62 | convolution fusion | flops 3166208 | bytes 535040 | tf_op jit(solution)/shard_map/sjihg,sihgp->sjhgp/dot_general | solution.py:136
  92.0 0.6 multiply_reduce_fusion
  92.6 0.9 reshape.335
  93.6 3.2 %copy.155 = bf16[4,2,8,64,256]{4,3,2,1,0:T(8,128)(2,1)} copy(bf16[4,2,8,64,256]{4,3,1,2,0:T(8,128)(2,1)} %bitcast.123) | data formatting | bytes 4194304 | tf_op jit(solution)/shard_map/transpose | solution.py:148
  96.7 15.9 %psum.7 = f32[128]{0:T(128)S(1)} all-reduce(f32[128]{0:T(128)S(1)} %reduce_sum.22), channel_id=1, replica_groups=mesh['grp'=2,'dp'=2,'kv'=4,'tp'=2] {'kv','tp'}, use_global_device_ids=true, to_apply=%region_2.4 | all-reduce | flops 128 | bytes 1024 | tf_op jit(solution)/shard_map/psum | solution.py:153
  112.6 3.1 %all-gather.2.cloned.1.call-done = bf16[128,4096]{1,0:T(8,128)(2,1)} async-done(((bf16[128,512]{1,0:T(8,128)(2,1)}), bf16[128,4096]{1,0:T(8,128)(2,1)}) %all-gather.2.cloned.1.call-update) | async-done | bytes 1048592 | tf_op jit(solution)/shard_map/all_gather | solution.py:155
  115.7 2.4 %fusion.12 = bf16[128,256]{1,0:T(8,128)(2,1)S(1)} fusion(bf16[128,4096]{1,0:T(8,128)(2,1)} %all-gather.2.cloned.1.call-done, bf16[4096,256]{1,0:T(8,128)(2,1)} %bitcast.121, f32[128]{0:T(128)S(1)} %add_rsqrt_fusion.1), kind=kOutput, calls=%fused_computation.24 | convolution fusion | flops 268500992 | bytes 3211776 | tf_op jit(solution)/shard_map/dot_general | solution.py:154
  118.1 0.7 reshape.338
  (101 shorter events, 2.9 us)
Async XLA Ops:
  6.5 33.1 %copy-start = (bf16[2048,8,1,64]{0,3,2,1:T(8,128)(2,1)S(1)}, bf16[2048,8,1,64]{0,3,2,1:T(8,128)(2,1)}, u32[]{:S(2)}) copy-start(bf16[2048,8,1,64]{0,3,2,1:T(8,128)(2,1)} %param.25) | copy-start | bytes 6291460
  6.5 0.8 copy-start.1
  6.5 109.2 %all-gather.2.cloned.1.call-start = ((), (), s32[]{:S(2)}) async-start(), calls=%async_computation | async-start | bytes 1179648 | tf_op jit(solution)/shard_map/all_gather | solution.py:155
  11.3 1.9 %copy-start.16 = (bf16[2048]{0:T(1024)(128)(2,1)S(1)}, bf16[2048]{0:T(1024)(128)(2,1)}, u32[]{:S(2)}) copy-start(bf16[2048]{0:T(1024)(128)(2,1)} %param.24) | copy-start | bytes 12292
  11.3 2.0 %copy-start.7 = (bf16[32,4,256]{2,1,0:T(4,128)(2,1)S(1)}, bf16[32,4,256]{2,1,0:T(4,128)(2,1)}, u32[]{:S(2)}) copy-start(bf16[32,4,256]{2,1,0:T(4,128)(2,1)} %param.23) | copy-start | bytes 196612
  39.7 3.3 %copy-start.25 = (s32[32]{0:T(128)S(1)}, s32[32]{0:T(128)}, u32[]{:S(2)}) copy-start(s32[32]{0:T(128)} %param.42) | copy-start | bytes 388
  39.7 4.7 %copy-start.14 = (f32[4,8,1,64]{3,2,1,0:T(1,128)S(1)}, f32[4,8,1,64]{3,2,1,0:T(1,128)}, u32[]{:S(2)}) copy-start(f32[4,8,1,64]{3,2,1,0:T(1,128)} %param.30) | copy-start | bytes 24580
  46.1 1.8 %copy-start.4 = (f32[32,4,512]{2,1,0:T(4,128)S(1)}, f32[32,4,512]{2,1,0:T(4,128)}, u32[]{:S(2)}) copy-start(f32[32,4,512]{2,1,0:T(4,128)} %fusion.68) | copy-start | bytes 786436
  46.1 1.8 %copy-start.12 = (s32[32,4]{1,0:T(8,128)S(1)}, s32[32,4]{1,0:T(8,128)}, u32[]{:S(2)}) copy-start(s32[32,4]{1,0:T(8,128)} %copy.134) | copy-start | bytes 1540
  48.0 2.9 %copy-start.17 = (f32[4,1,128]{2,1,0:T(1,128)S(1)}, f32[4,1,128]{2,1,0:T(1,128)}, u32[]{:S(2)}) copy-start(f32[4,1,128]{2,1,0:T(1,128)} %param.31) | copy-start | bytes 6148
  48.0 3.5 %copy-start.18 = (f32[4,1,128]{2,1,0:T(1,128)S(1)}, f32[4,1,128]{2,1,0:T(1,128)}, u32[]{:S(2)}) copy-start(f32[4,1,128]{2,1,0:T(1,128)} %param.32) | copy-start | bytes 6148
  48.0 4.1 %copy-start.11 = (f32[32,4,8,1]{0,3,2,1:T(1,128)S(1)}, f32[32,4,8,1]{0,3,2,1:T(1,128)}, u32[]{:S(2)}) copy-start(f32[32,4,8,1]{0,3,2,1:T(1,128)} %param.43) | copy-start | bytes 12292
  48.4 5.1 %copy-start.19 = (f32[8,1]{0,1:T(1,128)S(1)}, f32[8,1]{0,1:T(1,128)}, u32[]{:S(2)}) copy-start(f32[8,1]{0,1:T(1,128)} %param.33) | copy-start | bytes 100
  49.6 9.4 %copy-start.9 = (f32[32,4,128]{2,1,0:T(4,128)S(1)}, f32[32,4,128]{2,1,0:T(4,128)}, u32[]{:S(2)}) copy-start(f32[32,4,128]{2,1,0:T(4,128)} %fusion.75) | copy-start | bytes 196612
  53.1 7.6 %copy-start.13 = (s32[32,4]{1,0:T(8,128)S(1)}, s32[32,4]{1,0:T(8,128)}, u32[]{:S(2)}) copy-start(s32[32,4]{1,0:T(8,128)} %copy.134) | copy-start | bytes 1540
  53.1 7.6 %copy-start.20 = (f32[128]{0:T(128)S(1)}, f32[128]{0:T(128)}, u32[]{:S(2)}) copy-start(f32[128]{0:T(128)} %get-tuple-element.28) | copy-start | bytes 1540
  53.4 7.0 %copy-start.21 = (f32[128]{0:T(128)S(1)}, f32[128]{0:T(128)}, u32[]{:S(2)}) copy-start(f32[128]{0:T(128)} %get-tuple-element.31) | copy-start | bytes 1540
  54.5 5.6 %copy-start.22 = (f32[128]{0:T(128)S(1)}, f32[128]{0:T(128)}, u32[]{:S(2)}) copy-start(f32[128]{0:T(128)} %get-tuple-element.29) | copy-start | bytes 1540
  54.5 5.7 %copy-start.24 = (bf16[32,7,1,128]{3,0,2,1:T(8,128)(2,1)S(1)}, bf16[32,7,1,128]{3,0,2,1:T(8,128)(2,1)}, u32[]{:S(2)}) copy-start(bf16[32,7,1,128]{3,0,2,1:T(8,128)(2,1)} %param.40) | copy-start | bytes 172036
  54.5 5.7 %copy-start.28 = (f32[32,4,128]{2,1,0:T(4,128)S(1)}, f32[32,4,128]{2,1,0:T(4,128)}, u32[]{:S(2)}) copy-start(f32[32,4,128]{2,1,0:T(4,128)} %fusion.72) | copy-start | bytes 196612
  54.5 5.9 %copy-start.27 = (f32[32,4,128]{2,1,0:T(4,128)S(1)}, f32[32,4,128]{2,1,0:T(4,128)}, u32[]{:S(2)}) copy-start(f32[32,4,128]{2,1,0:T(4,128)} %fusion.69) | copy-start | bytes 196612
  54.5 6.2 %copy-start.26 = (f32[32,4,128]{2,1,0:T(4,128)S(1)}, f32[32,4,128]{2,1,0:T(4,128)}, u32[]{:S(2)}) copy-start(f32[32,4,128]{2,1,0:T(4,128)} %fusion.66) | copy-start | bytes 196612
  61.0 3.3 %copy-start.6 = (f32[32,4,128]{2,1,0:T(4,128)}, f32[32,4,128]{2,1,0:T(4,128)S(1)}, u32[]{:S(2)}) copy-start(f32[32,4,128]{2,1,0:T(4,128)S(1)} %divide_multiply_fusion.1) | copy-start | bytes 196612
  67.7 22.1 %copy-start.3 = (f32[32,4,8,64]{3,2,1,0:T(8,128)S(1)}, f32[32,4,8,64]{3,2,1,0:T(8,128)}, u32[]{:S(2)}) copy-start(f32[32,4,8,64]{3,2,1,0:T(8,128)} %reshape.321) | copy-start | bytes 786436
  67.7 22.1 %copy-start.5 = (f32[32,4,8]{1,2,0:T(8,128)S(1)}, f32[32,4,8]{1,2,0:T(8,128)}, u32[]{:S(2)}) copy-start(f32[32,4,8]{1,2,0:T(8,128)} %copy.151) | copy-start | bytes 12292
  67.7 22.1 %copy-start.10 = (f32[32,4,4]{2,1,0:T(4,128)S(1)}, f32[32,4,4]{2,1,0:T(4,128)}, u32[]{:S(2)}) copy-start(f32[32,4,4]{2,1,0:T(4,128)} %copy.149) | copy-start | bytes 6148
  67.7 22.1 %copy-start.15 = (pred[32,4,4]{2,1,0:T(4,128)(4,1)S(1)}, pred[32,4,4]{2,1,0:T(4,128)(4,1)}, u32[]{:S(2)}) copy-start(pred[32,4,4]{2,1,0:T(4,128)(4,1)} %fusion.90) | copy-start | bytes 1540
  89.8 2.2 %copy-start.2 = (f32[32,4,8,1,64]{4,2,3,1,0:T(8,128)S(1)}, f32[32,4,8,1,64]{4,2,3,1,0:T(8,128)}, u32[]{:S(2)}) copy-start(f32[32,4,8,1,64]{4,2,3,1,0:T(8,128)} %reshape.341) | copy-start | bytes 786436
  89.8 2.2 %copy-start.8 = (f32[32,4,8]{2,1,0:T(4,128)S(1)}, f32[32,4,8]{2,1,0:T(4,128)}, u32[]{:S(2)}) copy-start(f32[32,4,8]{2,1,0:T(4,128)} %get-tuple-element.35) | copy-start | bytes 12292
  89.8 2.2 %copy-start.23 = (f32[8,1]{0,1:T(1,128)S(1)}, f32[8,1]{0,1:T(1,128)}, u32[]{:S(2)}) copy-start(f32[8,1]{0,1:T(1,128)} %param.35) | copy-start | bytes 100
Sparse Core Ops, SparseCore 0:
  93.6 22.0 all-gather.1
where the time goes:
time: 126 us
  matrix products  52.5 us (42%)
  blocking collectives  31.3 us (25%)
  local copies, waits for them, and re-layouts  21.2 us (17%)
  between operations  14 us (11%)
  other arithmetic  3.44 us (3%)
  waiting for transfers between devices  3.11 us (2%)
    dot_general x1, matrix products, shards(): jnp.einsum('shgpn,sjgn->sjhgp', hidden_carried_memory, c_conv, precision=...  22.1 us
    psum x1, blocking collectives, shards(): sumsq_start = lax.psum(jnp.sum(gated_f * gated_f, axis=1), ('kv', 'tp'))  15.9 us
    all_gather x1, blocking collectives, shards(): piece = lax.all_gather(candidate_vectors, ('kv', 'tp'), axis=2, tiled=True)  15.4 us
    dot_general x12, matrix products, conv_tree(): value = jnp.einsum('sji,sic->sjc', onehots[lag], cur_f, precision=HIGH)  9.14 us
    dot_general x12, matrix products, conv_tree(): value = value + jnp.einsum('sjw,swc->sjc', chosen, saved_f, precision=HIGH)  8.55 us
    dot_general x5, matrix products, partial_dot(): return jnp.dot(source, weight, preferred_element_type=jnp.float32)  6.15 us
    gather x15, local copies, waits for them, and re-layouts, lineage_tables(): jnp.take_along_axis(predecessor_index, jnp.maximum(current, 0), axis=1)  5.63 us
    transpose x1, local copies, waits for them, and re-layouts, shards(): jnp.transpose(final_linear_matrix.reshape(kv_count, heads_dev, G, HD, out...  3.17 us
  transfers between devices with their start and end apart: 1, of which 1 were waited for; matrix products, arithmetic and copies ran while one was open for 3% of the time, Pallas kernels for 0%

commit v1 on v0

--- a/solution.py
+++ b/solution.py
@@ -150,7 +150,7 @@
     ).reshape(HG * G * HD, out_cols)
     empty = jnp.zeros((rows, out_cols), jnp.float32)
     gated_f = gated.astype(jnp.float32)
-    sumsq_start = lax.psum(jnp.sum(gated_f * gated_f, axis=1), ("kv", "tp"))
+    sumsq_start = lax.psum(lax.psum(jnp.sum(gated_f * gated_f, axis=1), "tp"), "kv")
     product = jnp.dot(
         lax.all_gather(gated, ("kv", "tp"), axis=1, tiled=True),
         out_flat,

time: 126 us -> 126 us (level)
  waiting for transfers between devices: 3.11 us -> 5.59 us
  blocking collectives: 31.3 us -> 28.9 us
    all_gather x1, waiting for transfers between devices: 3.1 us -> 5.58 us  [shards(): lax.all_gather(gated, ('kv', 'tp'), axis=1, tiled=True)]
    psum x1 -> x2, blocking collectives: 15.9 us -> 13.5 us  [the longest x1 11 us: shards(): lax.psum(lax.psum(jnp.sum(gated_f * gated_f, axis=1), 'tp'), 'kv')]
where the time goes in v1:
time: 126 us
  matrix products  52.5 us (42%)
  blocking collectives  28.9 us (23%)
  local copies, waits for them, and re-layouts  21.2 us (17%)
  between operations  14 us (11%)
  waiting for transfers between devices  5.59 us (4%)
  other arithmetic  3.43 us (3%)
    dot_general x1, matrix products, shards(): jnp.einsum('shgpn,sjgn->sjhgp', hidden_carried_memory, c_conv, precision=...  22.1 us
    all_gather x1, blocking collectives, shards(): piece = lax.all_gather(candidate_vectors, ('kv', 'tp'), axis=2, tiled=True)  15.4 us
    psum x1, blocking collectives, shards(): lax.psum(lax.psum(jnp.sum(gated_f * gated_f, axis=1), 'tp'), 'kv')  11 us
    dot_general x12, matrix products, conv_tree(): value = jnp.einsum('sji,sic->sjc', onehots[lag], cur_f, precision=HIGH)  9.1 us
    dot_general x12, matrix products, conv_tree(): value = value + jnp.einsum('sjw,swc->sjc', chosen, saved_f, precision=HIGH)  8.55 us
    dot_general x5, matrix products, partial_dot(): return jnp.dot(source, weight, preferred_element_type=jnp.float32)  6.16 us
    gather x15, local copies, waits for them, and re-layouts, lineage_tables(): jnp.take_along_axis(predecessor_index, jnp.maximum(current, 0), axis=1)  5.63 us
    all_gather x1, waiting for transfers between devices, shards(): lax.all_gather(gated, ('kv', 'tp'), axis=1, tiled=True)  5.58 us
  transfers between devices with their start and end apart: 1, of which 1 were waited for; matrix products, arithmetic and copies ran while one was open for 3% of the time, Pallas kernels for 0%

profile of v1, /device:TPU:0, one launch (start us, length us, event | category | flops | bytes accessed | tf_op | source)
XLA Modules:
  0.0 125.6 jit_solution(15674079285626815604)
XLA Ops:
  6.8 0.5 copy-done.1
  7.4 1.5 %gather_fusion = s32[128]{0:T(128)S(1)} fusion(s32[32,4]{0,1:T(4,128)S(1)} %copy-done.1, s32[128]{0:T(128)S(1)} %reshape.376), kind=kCustom, calls=%fused_computation.clone | custom fusion | bytes 2048 | tf_op jit(solution)/shard_map/jit(take_along_axis)/gather | solution.py:26
  9.2 0.1 reshape.381
  9.4 1.5 %gather_fusion.1 = s32[128]{0:T(128)S(1)} fusion(s32[32,4]{0,1:T(4,128)S(1)} %copy-done.1, s32[128]{0:T(128)S(1)} %reshape.381), kind=kCustom, calls=%fused_computation.1.clone | custom fusion | bytes 2048 | tf_op jit(solution)/shard_map/jit(take_along_axis)/gather | solution.py:26
  11.2 0.1 reshape.386
  11.3 1.5 %gather_fusion.2 = s32[128]{0:T(128)S(1)} fusion(s32[32,4]{0,1:T(4,128)S(1)} %copy-done.1, s32[128]{0:T(128)S(1)} %reshape.386), kind=kCustom, calls=%fused_computation.2.clone | custom fusion | bytes 2048 | tf_op jit(solution)/shard_map/jit(take_along_axis)/gather | solution.py:26
  13.3 15.4 %all_gather.6 = bf16[32,4,2048]{2,1,0:T(4,128)(2,1)S(1)} all-gather(bf16[32,4,256]{2,1,0:T(4,128)(2,1)S(1)} %copy-done.7), channel_id=1, replica_groups=mesh['grp'=2,'dp'=2,'kv'=4,'tp'=2] {'kv','tp'}, dimensions={2}, use_global_device_ids=true | all-gather | bytes 589824 | tf_op jit(solution)/shard_map/all_gather | solution.py:82
  28.7 0.5 fusion.30
  29.4 0.1 reshape.317
  29.5 1.3 %fusion.27 = bf16[128,128]{1,0:T(8,128)(2,1)S(1)} fusion(bf16[128,2048]{1,0:T(8,128)(2,1)S(1)} %reshape.317, bf16[2048,1,128]{2,0,1:T(8,128)(2,1)} %param.28, f32[128]{0:T(128)S(1)} %rsqrt.14), kind=kOutput, calls=%fused_computation.50 | convolution fusion | flops 67141632 | bytes 1081856 | tf_op jit(solution)/shard_map/dot_general | solution.py:89
  30.9 0.9 fusion.67
  31.7 0.8 fusion.70
  32.6 0.8 fusion.90
  33.4 0.8 fusion.73
  34.2 0.8 fusion.76
  35.0 1.3 %fusion.28 = bf16[128,128]{1,0:T(8,128)(2,1)S(1)} fusion(bf16[128,2048]{1,0:T(8,128)(2,1)S(1)} %reshape.317, bf16[2048,1,128]{2,0,1:T(8,128)(2,1)} %param.29, f32[128]{0:T(128)S(1)} %rsqrt.14), kind=kOutput, calls=%fused_computation.51 | convolution fusion | flops 67141632 | bytes 1081856 | tf_op jit(solution)/shard_map/dot_general | solution.py:89
  36.3 0.8 fusion.66
  37.2 0.8 fusion.69
  38.0 0.8 fusion.72
  38.9 0.8 fusion.75
  39.7 0.8 fusion.9
  40.5 1.0 fusion.68
  41.5 0.3 fusion.71
  41.8 1.0 fusion.74
  42.8 0.2 fusion.77
  43.4 0.7 copy.134
  44.7 1.3 %reshape.391 = bf16[32,7,512]{2,1,0:T(8,128)(2,1)S(1)} reshape(bf16[32,7,8,1,64]{4,2,3,1,0:T(8,128)(2,1)} %param.38) | data formatting | bytes 458752 | tf_op jit(solution)/shard_map/reshape | solution.py:106
  46.1 0.3 fusion.8
  46.4 1.2 fusion.7
  47.6 0.3 fusion.5
  48.0 0.4 divide_multiply_fusion
  48.4 0.2 reshape.333
  48.6 1.0 reshape.321
  49.6 1.2 negate_bitcast_fusion
  50.8 0.6 slice_bitcast_fusion.4
  51.4 0.6 slice_bitcast_fusion
  52.1 0.9 constant_dynamic-slice_fusion
  53.0 0.2 convolution_multiply_fusion.5
  53.3 0.1 copy.137
  53.5 0.9 copy.151
  54.4 1.1 fusion.26
  55.6 1.1 fusion.25
  56.7 1.1 fusion.23
  57.8 1.2 fusion.21
  59.0 1.1 fusion.19
  60.1 0.3 fusion.18
  60.4 0.3 fusion.16
  60.7 0.3 divide_multiply_fusion.1
  60.9 0.4 convolution_bitcast_fusion
  61.3 0.9 copy.149
  62.2 1.7 %fusion.124 = (f32[32,4,8]{2,1,0:T(4,128)}, f32[32,4,8]{2,1,0:T(4,128)S(1)}) fusion(f32[32,4,8,1]{2,1,0,3:T(4,128)S(1)} %copy.138, f32[32,4,8,1]{2,1,0,3:T(4,128)S(1)} %bitcast.125, f32[8]{0:T(128)S(1)} %bitcast.135, f32[8]{0:T(128)} %negate_bitcast_fusion, s32[32,4]{1,0:T(8,128)S(1)} %copy.132, s32[32,4]{1,0:T(8,128)S(1)} %copy.128, s32[32,4]{1,0:T(8,128)S(1)} %copy.124), kind=kOutput, calls=%fused_computation.189 | convolution fusion | flops 64000 | bytes 17984 | tf_op jit(solution)/shard_map/sji,sihg->sjhg/dot_general | solution.py:131
  64.0 0.3 copy.139
  64.2 2.4 %fusion.11 = f32[128,512]{1,0:T(8,128)S(1)} fusion(bf16[128,2048]{1,0:T(8,128)(2,1)S(1)} %reshape.317, bf16[2048,512]{0,1:T(8,128)(2,1)} %bitcast.122, f32[128]{0:T(128)S(1)} %rsqrt.14), kind=kOutput, calls=%fused_computation.22 | convolution fusion | flops 268632064 | bytes 2884096 | tf_op jit(solution)/shard_map/dot_general | solution.py:89
  66.7 0.9 reshape.341
  67.6 22.1 %fusion = f32[32,4,8,64]{3,1,2,0:T(4,128)S(1)} fusion(f32[32,8,1,64,128]{4,3,2,1,0:T(8,128)} %param.37, f32[32,4,128]{2,1,0:T(4,128)} %copy-done.6), kind=kOutput, calls=%fused_computation.3 | convolution fusion | flops 100663296 | bytes 8716288 | tf_op jit(solution)/shard_map/shgpn,sjgn->sjhgp/dot_general | solution.py:137
  89.8 2.1 %fusion.36 = f32[32,8,64,4]{2,3,1,0:T(4,128)S(1)} fusion(f32[32,4,8,64]{3,2,1,0:T(8,128)S(1)} %copy-done.3, f32[32,4,8]{1,2,0:T(8,128)S(1)} %copy-done.5, f32[32,4,4]{2,1,0:T(4,128)S(1)} %copy-done.10, f32[32,4,8]{1,2,0:T(8,128)S(1)} %copy.139, pred[32,4,4]{2,1,0:T(4,128)(4,1)S(1)} %copy-done.15), kind=kOutput, calls=%fused_computation.62 | convolution fusion | flops 3166208 | bytes 535040 | tf_op jit(solution)/shard_map/sjihg,sihgp->sjhgp/dot_general | solution.py:136
  91.9 0.6 multiply_reduce_fusion
  92.5 0.9 reshape.335
  93.5 3.2 %copy.155 = bf16[4,2,8,64,256]{4,3,2,1,0:T(8,128)(2,1)} copy(bf16[4,2,8,64,256]{4,3,1,2,0:T(8,128)(2,1)} %bitcast.123) | data formatting | bytes 4194304 | tf_op jit(solution)/shard_map/transpose | solution.py:148
  96.7 2.5 %psum.14 = f32[128]{0:T(128)S(1)} all-reduce(f32[128]{0:T(128)S(1)} %reduce_sum.22), channel_id=1, replica_groups=mesh['grp'=2,'dp'=2,'kv'=4,'tp'=2] {'tp'}, use_global_device_ids=true, to_apply=%region_2.4 | all-reduce | flops 128 | bytes 1024 | tf_op jit(solution)/shard_map/psum | solution.py:153
  99.1 11.0 %psum.15 = f32[128]{0:T(128)S(1)} all-reduce(f32[128]{0:T(128)S(1)} %psum.14), channel_id=1, replica_groups=mesh['grp'=2,'dp'=2,'kv'=4,'tp'=2] {'kv'}, use_global_device_ids=true, to_apply=%region_3.5 | all-reduce | flops 128 | bytes 1024 | tf_op jit(solution)/shard_map/psum | solution.py:153
  110.2 5.6 %all-gather.2.cloned.1.call-done = bf16[128,4096]{1,0:T(8,128)(2,1)} async-done(((bf16[128,512]{1,0:T(8,128)(2,1)}), bf16[128,4096]{1,0:T(8,128)(2,1)}) %all-gather.2.cloned.1.call-update) | async-done | bytes 1048592 | tf_op jit(solution)/shard_map/all_gather | solution.py:155
  115.7 2.4 %fusion.12 = bf16[128,256]{1,0:T(8,128)(2,1)S(1)} fusion(bf16[128,4096]{1,0:T(8,128)(2,1)} %all-gather.2.cloned.1.call-done, bf16[4096,256]{1,0:T(8,128)(2,1)} %bitcast.121, f32[128]{0:T(128)S(1)} %add_rsqrt_fusion.1), kind=kOutput, calls=%fused_computation.24 | convolution fusion | flops 268500992 | bytes 3211776 | tf_op jit(solution)/shard_map/dot_general | solution.py:154
  118.1 0.7 reshape.338
  (102 shorter events, 3.0 us)
Async XLA Ops:
  6.5 33.1 %copy-start = (bf16[2048,8,1,64]{0,3,2,1:T(8,128)(2,1)S(1)}, bf16[2048,8,1,64]{0,3,2,1:T(8,128)(2,1)}, u32[]{:S(2)}) copy-start(bf16[2048,8,1,64]{0,3,2,1:T(8,128)(2,1)} %param.25) | copy-start | bytes 6291460
  6.5 0.8 copy-start.1
  6.5 109.2 %all-gather.2.cloned.1.call-start = ((), (), s32[]{:S(2)}) async-start(), calls=%async_computation | async-start | bytes 1179648 | tf_op jit(solution)/shard_map/all_gather | solution.py:155
  11.3 1.9 %copy-start.16 = (bf16[2048]{0:T(1024)(128)(2,1)S(1)}, bf16[2048]{0:T(1024)(128)(2,1)}, u32[]{:S(2)}) copy-start(bf16[2048]{0:T(1024)(128)(2,1)} %param.24) | copy-start | bytes 12292
  11.3 2.0 %copy-start.7 = (bf16[32,4,256]{2,1,0:T(4,128)(2,1)S(1)}, bf16[32,4,256]{2,1,0:T(4,128)(2,1)}, u32[]{:S(2)}) copy-start(bf16[32,4,256]{2,1,0:T(4,128)(2,1)} %param.23) | copy-start | bytes 196612
  39.6 3.3 %copy-start.25 = (s32[32]{0:T(128)S(1)}, s32[32]{0:T(128)}, u32[]{:S(2)}) copy-start(s32[32]{0:T(128)} %param.42) | copy-start | bytes 388
  39.6 4.7 %copy-start.14 = (f32[4,8,1,64]{3,2,1,0:T(1,128)S(1)}, f32[4,8,1,64]{3,2,1,0:T(1,128)}, u32[]{:S(2)}) copy-start(f32[4,8,1,64]{3,2,1,0:T(1,128)} %param.30) | copy-start | bytes 24580
  46.1 1.8 %copy-start.4 = (f32[32,4,512]{2,1,0:T(4,128)S(1)}, f32[32,4,512]{2,1,0:T(4,128)}, u32[]{:S(2)}) copy-start(f32[32,4,512]{2,1,0:T(4,128)} %fusion.68) | copy-start | bytes 786436
  46.1 1.8 %copy-start.12 = (s32[32,4]{1,0:T(8,128)S(1)}, s32[32,4]{1,0:T(8,128)}, u32[]{:S(2)}) copy-start(s32[32,4]{1,0:T(8,128)} %copy.134) | copy-start | bytes 1540
  47.9 2.9 %copy-start.17 = (f32[4,1,128]{2,1,0:T(1,128)S(1)}, f32[4,1,128]{2,1,0:T(1,128)}, u32[]{:S(2)}) copy-start(f32[4,1,128]{2,1,0:T(1,128)} %param.31) | copy-start | bytes 6148
  47.9 3.5 %copy-start.18 = (f32[4,1,128]{2,1,0:T(1,128)S(1)}, f32[4,1,128]{2,1,0:T(1,128)}, u32[]{:S(2)}) copy-start(f32[4,1,128]{2,1,0:T(1,128)} %param.32) | copy-start | bytes 6148
  48.0 4.0 %copy-start.11 = (f32[32,4,8,1]{0,3,2,1:T(1,128)S(1)}, f32[32,4,8,1]{0,3,2,1:T(1,128)}, u32[]{:S(2)}) copy-start(f32[32,4,8,1]{0,3,2,1:T(1,128)} %param.43) | copy-start | bytes 12292
  48.3 5.1 %copy-start.19 = (f32[8,1]{0,1:T(1,128)S(1)}, f32[8,1]{0,1:T(1,128)}, u32[]{:S(2)}) copy-start(f32[8,1]{0,1:T(1,128)} %param.33) | copy-start | bytes 100
  49.6 9.4 %copy-start.9 = (f32[32,4,128]{2,1,0:T(4,128)S(1)}, f32[32,4,128]{2,1,0:T(4,128)}, u32[]{:S(2)}) copy-start(f32[32,4,128]{2,1,0:T(4,128)} %fusion.75) | copy-start | bytes 196612
  53.0 7.6 %copy-start.13 = (s32[32,4]{1,0:T(8,128)S(1)}, s32[32,4]{1,0:T(8,128)}, u32[]{:S(2)}) copy-start(s32[32,4]{1,0:T(8,128)} %copy.134) | copy-start | bytes 1540
  53.0 7.6 %copy-start.20 = (f32[128]{0:T(128)S(1)}, f32[128]{0:T(128)}, u32[]{:S(2)}) copy-start(f32[128]{0:T(128)} %get-tuple-element.28) | copy-start | bytes 1540
  53.4 7.0 %copy-start.21 = (f32[128]{0:T(128)S(1)}, f32[128]{0:T(128)}, u32[]{:S(2)}) copy-start(f32[128]{0:T(128)} %get-tuple-element.31) | copy-start | bytes 1540
  54.4 5.6 %copy-start.22 = (f32[128]{0:T(128)S(1)}, f32[128]{0:T(128)}, u32[]{:S(2)}) copy-start(f32[128]{0:T(128)} %get-tuple-element.29) | copy-start | bytes 1540
  54.4 5.7 %copy-start.24 = (bf16[32,7,1,128]{3,0,2,1:T(8,128)(2,1)S(1)}, bf16[32,7,1,128]{3,0,2,1:T(8,128)(2,1)}, u32[]{:S(2)}) copy-start(bf16[32,7,1,128]{3,0,2,1:T(8,128)(2,1)} %param.40) | copy-start | bytes 172036
  54.4 5.7 %copy-start.28 = (f32[32,4,128]{2,1,0:T(4,128)S(1)}, f32[32,4,128]{2,1,0:T(4,128)}, u32[]{:S(2)}) copy-start(f32[32,4,128]{2,1,0:T(4,128)} %fusion.72) | copy-start | bytes 196612
  54.4 5.9 %copy-start.27 = (f32[32,4,128]{2,1,0:T(4,128)S(1)}, f32[32,4,128]{2,1,0:T(4,128)}, u32[]{:S(2)}) copy-start(f32[32,4,128]{2,1,0:T(4,128)} %fusion.69) | copy-start | bytes 196612
  54.4 6.2 %copy-start.26 = (f32[32,4,128]{2,1,0:T(4,128)S(1)}, f32[32,4,128]{2,1,0:T(4,128)}, u32[]{:S(2)}) copy-start(f32[32,4,128]{2,1,0:T(4,128)} %fusion.66) | copy-start | bytes 196612
  60.9 3.3 %copy-start.6 = (f32[32,4,128]{2,1,0:T(4,128)}, f32[32,4,128]{2,1,0:T(4,128)S(1)}, u32[]{:S(2)}) copy-start(f32[32,4,128]{2,1,0:T(4,128)S(1)} %divide_multiply_fusion.1) | copy-start | bytes 196612
  67.6 22.1 %copy-start.3 = (f32[32,4,8,64]{3,2,1,0:T(8,128)S(1)}, f32[32,4,8,64]{3,2,1,0:T(8,128)}, u32[]{:S(2)}) copy-start(f32[32,4,8,64]{3,2,1,0:T(8,128)} %reshape.321) | copy-start | bytes 786436
  67.6 22.1 %copy-start.5 = (f32[32,4,8]{1,2,0:T(8,128)S(1)}, f32[32,4,8]{1,2,0:T(8,128)}, u32[]{:S(2)}) copy-start(f32[32,4,8]{1,2,0:T(8,128)} %copy.151) | copy-start | bytes 12292
  67.6 22.1 %copy-start.10 = (f32[32,4,4]{2,1,0:T(4,128)S(1)}, f32[32,4,4]{2,1,0:T(4,128)}, u32[]{:S(2)}) copy-start(f32[32,4,4]{2,1,0:T(4,128)} %copy.149) | copy-start | bytes 6148
  67.6 22.1 %copy-start.15 = (pred[32,4,4]{2,1,0:T(4,128)(4,1)S(1)}, pred[32,4,4]{2,1,0:T(4,128)(4,1)}, u32[]{:S(2)}) copy-start(pred[32,4,4]{2,1,0:T(4,128)(4,1)} %fusion.90) | copy-start | bytes 1540
  89.7 2.2 %copy-start.2 = (f32[32,4,8,1,64]{4,2,3,1,0:T(8,128)S(1)}, f32[32,4,8,1,64]{4,2,3,1,0:T(8,128)}, u32[]{:S(2)}) copy-start(f32[32,4,8,1,64]{4,2,3,1,0:T(8,128)} %reshape.341) | copy-start | bytes 786436
  89.7 2.2 %copy-start.8 = (f32[32,4,8]{2,1,0:T(4,128)S(1)}, f32[32,4,8]{2,1,0:T(4,128)}, u32[]{:S(2)}) copy-start(f32[32,4,8]{2,1,0:T(4,128)} %get-tuple-element.35) | copy-start | bytes 12292
  89.8 2.2 %copy-start.23 = (f32[8,1]{0,1:T(1,128)S(1)}, f32[8,1]{0,1:T(1,128)}, u32[]{:S(2)}) copy-start(f32[8,1]{0,1:T(1,128)} %param.35) | copy-start | bytes 100
Sparse Core Ops, SparseCore 0:
  93.5 22.2 all-gather.1
